TPU v7x, 32 devices: a whole 2x2x4 slice. The times are simulated.
32 devices in a mesh: row: 16 (over z, y, x), col: 2 (over core).
Axes of the slice: x: 2, y: 2, z: 4, core: 2. Of those that a mesh axis runs over, the one named last changes fastest.
Arguments:
- tokens: bfloat16 [2, 6144, 2048], P('col', 'row'), may hold values from -6 to 6
- norm_gain: bfloat16 [2048], replicated, may hold values from 0.099609375 to 1.8984375
- in_weight: bfloat16 [2048, 512], P('row', 'col'), may hold values from -0.125 to 0.125
- out_weight: bfloat16 [512, 2048], P('col', 'row'), may hold values from -0.25 to 0.25
Outputs:
- mixed: bfloat16 [2, 6144, 2048], P('col', 'row')
All inputs are finite; a program needn't handle non-finite values.
Results may differ from a plain program's by a relative error of at most 0.013.
Values may be sent and summed in bfloat16 or wider, within the bound.
A program may use at most 64 MiB of HBM per device.

v0:
```python
import math

import jax
import jax.numpy as jnp
from jax import lax
from jax.sharding import PartitionSpec as P

GS = 64


EPS = 1e-06
PRECISE = lax.Precision.HIGHEST


def angle_pair(left_index, right_index, modulus):
    product = left_index[:, None] * right_index[None, :] % modulus
    radians = product.astype(jnp.float32) * (2.0 * math.pi / modulus)
    return (jnp.cos(radians), jnp.sin(radians))


def table_dot(matrix, values):
    return jnp.dot(matrix, values, precision=PRECISE, preferred_element_type=jnp.float32)


def right_dot(values, matrix):
    return jnp.dot(values, matrix, precision=PRECISE, preferred_element_type=jnp.float32)


def body(tokens, norm_gain, in_weight, out_weight):
    own_rows = tokens[0].astype(jnp.float32)
    inverse_rms = lax.rsqrt(jnp.mean(own_rows * own_rows, axis=-1, keepdims=True) + EPS)
    normed = (own_rows * inverse_rms * norm_gain.astype(jnp.float32)).astype(jnp.bfloat16)
    in_columns, out_rows = (
        lax.all_gather(in_weight, "col", axis=1, tiled=True),
        lax.all_gather(out_weight, "col", axis=0, tiled=True),
    )
    row_count = normed.shape[0]
    channels = in_columns.shape[1]
    peer_count = lax.axis_size("row")
    length = row_count * peer_count
    projected = jnp.dot(
        normed,
        lax.all_gather(in_columns, "row", axis=0, tiled=True),
        preferred_element_type=jnp.float32,
    ).astype(jnp.bfloat16)
    channel_index = jnp.arange(channels, dtype=jnp.int32)
    within = channel_index % GS
    same_group = channel_index[:, None] // GS == channel_index[None, :] // GS
    group_cos, group_sin = angle_pair(within, within, GS)
    group_cos = jnp.where(same_group, group_cos, 0.0)
    group_sin = jnp.where(same_group, group_sin, 0.0)
    peer_index = jnp.arange(peer_count, dtype=jnp.int32)
    small_cos, small_sin = angle_pair(peer_index, peer_index, peer_count)
    line_index = jnp.arange(row_count, dtype=jnp.int32)
    long_cos, long_sin = angle_pair(line_index, line_index, row_count)
    gathered = lax.all_to_all(projected, "row", split_axis=1, concat_axis=0, tiled=True).astype(
        jnp.float32
    )
    narrow = gathered.shape[1]
    flat = gathered.reshape(peer_count, row_count * narrow)
    first_real = table_dot(small_cos, flat).reshape(peer_count, row_count, narrow)
    first_imag = (-table_dot(small_sin, flat)).reshape(peer_count, row_count, narrow)
    turn_cos, turn_sin = angle_pair(peer_index, line_index, length)
    turn_cos = turn_cos[:, :, None]
    turn_sin = turn_sin[:, :, None]
    turned_real = first_real * turn_cos + first_imag * turn_sin
    turned_imag = first_imag * turn_cos - first_real * turn_sin
    lines_real = turned_real.transpose(1, 0, 2).reshape(row_count, peer_count * narrow)
    lines_imag = turned_imag.transpose(1, 0, 2).reshape(row_count, peer_count * narrow)
    whole_real = (table_dot(long_cos, lines_real) + table_dot(long_sin, lines_imag)).reshape(
        length, narrow
    )
    whole_imag = (table_dot(long_cos, lines_imag) - table_dot(long_sin, lines_real)).reshape(
        length, narrow
    )
    back_real, back_imag = (
        lax.all_to_all(
            whole_real.astype(jnp.bfloat16), "row", split_axis=0, concat_axis=1, tiled=True
        ).astype(whole_real.dtype),
        lax.all_to_all(
            whole_imag.astype(jnp.bfloat16), "row", split_axis=0, concat_axis=1, tiled=True
        ).astype(whole_imag.dtype),
    )
    mixed_real = right_dot(back_real, group_cos) + right_dot(back_imag, group_sin)
    arranged = (mixed_real * (1.0 / math.sqrt(length * GS))).astype(jnp.bfloat16)
    result = jnp.dot(
        arranged,
        lax.all_gather(out_rows, "row", axis=1, tiled=True),
        preferred_element_type=jnp.float32,
    )
    return result.astype(jnp.bfloat16)[None]


def solution(mesh):
    in_specs = (P("col", "row", None), P(), P("row", "col"), P("col", "row"))
    out_specs = P("col", "row", None)
    return jax.shard_map(body, mesh=mesh, in_specs=in_specs, out_specs=out_specs, check_vma=False)
```

profile of v0, /device:TPU:0, one launch (start us, length us, event | category | flops | bytes accessed | tf_op | source)
XLA Modules:
  0.0 173.7 jit_solution(4385895782396429230)
XLA Ops:
  6.5 3.8 %all_gather.12 = bf16[128,512]{1,0:T(8,128)(2,1)} all-gather(bf16[128,256]{1,0:T(8,128)(2,1)} %param.6), channel_id=1, replica_groups=mesh['row'=16,'col'=2] {'col'}, dimensions={1}, use_global_device_ids=true | all-gather | bytes 196608 | tf_op jit(solution)/shard_map/all_gather | solution.py:34
  10.4 3.4 %all_gather.14 = bf16[512,128]{1,0:T(8,128)(2,1)} all-gather(bf16[256,128]{1,0:T(8,128)(2,1)} %param.7), channel_id=1, replica_groups=mesh['row'=16,'col'=2] {'col'}, dimensions={0}, use_global_device_ids=true | all-gather | bytes 196608 | tf_op jit(solution)/shard_map/all_gather | solution.py:35
  13.8 0.7 convert_element_type.77
  14.5 1.8 %fusion = f32[384]{0:T(512)S(1)} fusion(bf16[1,384,2048]{2,1,0:T(8,128)(2,1)} %param.4), kind=kLoop, calls=%fused_computation.3 | loop fusion | flops 2358912 | bytes 1574400 | tf_op jit(solution)/shard_map/reduce_sum | solution.py:31
  16.3 57.0 %all-gather.3.cloned.1.call-done = bf16[2048,512]{1,0:T(8,128)(2,1)} async-done(((bf16[128,512]{1,0:T(8,128)(2,1)}), bf16[2048,512]{1,0:T(8,128)(2,1)}) %all-gather.3.cloned.1.call-update) | async-done | bytes 2097168 | tf_op jit(solution)/shard_map/all_gather | solution.py:43
  73.3 2.6 %fusion.13 = bf16[384,512]{1,0:T(8,128)(2,1)S(1)} fusion(bf16[2048,512]{1,0:T(8,128)(2,1)} %all-gather.3.cloned.1.call-done, bf16[1,384,2048]{2,1,0:T(8,128)(2,1)S(1)} %copy-done.1, f32[2048]{0:T(1024)S(1)} %convert_element_type.77, f32[384]{0:T(512)S(1)} %add_rsqrt_fusion), kind=kOutput, calls=%fused_computation.26 | convolution fusion | flops 808648704 | bytes 4072960 | tf_op jit(solution)/shard_map/dot_general | solution.py:41
  75.9 0.9 copy.14
  76.9 4.4 %all-to-all-start = ((bf16[384,16,32]{0,2,1:T(8,128)(2,1)}), bf16[384,16,32]{0,2,1:T(8,128)(2,1)S(1)}, u32[]{:S(2)}, u32[]{:S(2)}) async-start(bf16[384,16,32]{0,2,1:T(8,128)(2,1)} %bitcast.3), calls=%async_computation | async-start | bytes 786432 | tf_op jit(solution)/shard_map/all_to_all | solution.py:56
  81.3 0.7 fusion.59
  82.0 10.8 %all-to-all-done = bf16[384,16,32]{0,2,1:T(8,128)(2,1)S(1)} async-done(((bf16[384,16,32]{0,2,1:T(8,128)(2,1)}), bf16[384,16,32]{0,2,1:T(8,128)(2,1)S(1)}, u32[]{:S(2)}, u32[]{:S(2)}) %all-to-all-start) | async-done | bytes 393248 | tf_op jit(solution)/shard_map/all_to_all | solution.py:56
  92.9 0.8 copy.15
  93.7 1.6 reshape.164
  95.3 1.4 convolution_negate_fusion
  96.7 2.2 %reshape.165 = f32[16,384,32]{2,1,0:T(8,128)S(1)} reshape(f32[16,12288]{1,0:T(8,128)} %convolution_negate_fusion) | data formatting | bytes 1572864 | tf_op jit(solution)/shard_map/reshape | solution.py:62
  98.9 1.9 %copy.17 = f32[16,384,32]{1,0,2:T(8,128)} copy(f32[16,384,32]{2,1,0:T(8,128)S(1)} %reshape.165) | data formatting | bytes 1572864 | tf_op jit(solution)/shard_map/reshape | solution.py:62
  100.8 1.3 dot_general.36
  102.1 0.7 copy.16
  104.1 5.1 %fusion.30 = f32[384,512]{1,0:T(8,128)S(1)} fusion(f32[384,512]{0,1:T(8,128)S(1)} %bitcast.46), kind=kOutput, calls=%fused_computation.44 | convolution fusion | flops 907296768 | bytes 1572864 | tf_op jit(solution)/shard_map/dot_general | solution.py:22
  109.2 4.3 %fusion.10 = bf16[384,512]{1,0:T(8,128)(2,1)S(1)} fusion(f32[384,512]{1,0:T(8,128)S(1)} %fusion.30, f32[384,512]{0,1:T(8,128)S(1)} %bitcast.48), kind=kOutput, calls=%fused_computation.23 | convolution fusion | flops 907689984 | bytes 1966080 | tf_op jit(solution)/shard_map/dot_general | solution.py:22
  113.5 0.9 convert_element_type.82
  114.4 1.3 copy.21
  115.7 3.7 %all-to-all-start.1 = ((bf16[16,384,32]{1,2,0:T(8,128)(2,1)}), bf16[16,384,32]{1,2,0:T(8,128)(2,1)S(1)}, u32[]{:S(2)}, u32[]{:S(2)}) async-start(bf16[16,384,32]{1,2,0:T(8,128)(2,1)} %copy.21), calls=%async_computation.1 | async-start | bytes 786432 | tf_op jit(solution)/shard_map/all_to_all | solution.py:77
  119.4 5.1 %fusion.28 = f32[384,512]{1,0:T(8,128)S(1)} fusion(f32[384,512]{0,1:T(8,128)S(1)} %bitcast.49), kind=kOutput, calls=%fused_computation.43 | convolution fusion | flops 907296768 | bytes 1572864 | tf_op jit(solution)/shard_map/dot_general | solution.py:22
  124.5 4.3 %fusion.11 = bf16[384,512]{1,0:T(8,128)(2,1)S(1)} fusion(f32[384,512]{1,0:T(8,128)S(1)} %fusion.28, f32[384,512]{0,1:T(8,128)S(1)} %bitcast.47), kind=kOutput, calls=%fused_computation.24 | convolution fusion | flops 907689984 | bytes 1966080 | tf_op jit(solution)/shard_map/dot_general | solution.py:22
  128.9 0.9 convert_element_type.85
  129.7 1.3 copy.22
  131.0 6.3 %all-to-all-done.1 = bf16[16,384,32]{1,2,0:T(8,128)(2,1)S(1)} async-done(((bf16[16,384,32]{1,2,0:T(8,128)(2,1)}), bf16[16,384,32]{1,2,0:T(8,128)(2,1)S(1)}, u32[]{:S(2)}, u32[]{:S(2)}) %all-to-all-start.1) | async-done | bytes 393248 | tf_op jit(solution)/shard_map/all_to_all | solution.py:77
  137.3 8.8 %all-to-all-start.2 = ((bf16[16,384,32]{1,2,0:T(8,128)(2,1)}), bf16[16,384,32]{1,2,0:T(8,128)(2,1)S(1)}, u32[]{:S(2)}, u32[]{:S(2)}) async-start(bf16[16,384,32]{1,2,0:T(8,128)(2,1)} %copy.22), calls=%async_computation.2 | async-start | bytes 786432 | tf_op jit(solution)/shard_map/all_to_all | solution.py:80
  146.2 4.8 %fusion.16 = f32[384,512]{1,0:T(8,128)S(1)} fusion(bf16[384,512]{0,1:T(8,128)(2,1)S(1)} %bitcast.50, s32[512]{0:T(512)S(1)} %get-tuple-element.9, s32[512]{0:T(512)S(1)} %get-tuple-element.10), kind=kOutput, calls=%fused_computation.27 | convolution fusion | flops 1212153856 | bytes 1183744 | tf_op jit(solution)/shard_map/dot_general | solution.py:26
  151.0 7.2 %all-to-all-done.2 = bf16[16,384,32]{1,2,0:T(8,128)(2,1)S(1)} async-done(((bf16[16,384,32]{1,2,0:T(8,128)(2,1)}), bf16[16,384,32]{1,2,0:T(8,128)(2,1)S(1)}, u32[]{:S(2)}, u32[]{:S(2)}) %all-to-all-start.2) | async-done | bytes 393248 | tf_op jit(solution)/shard_map/all_to_all | solution.py:80
  158.2 4.9 %fusion.12 = bf16[384,512]{1,0:T(8,128)(2,1)S(1)} fusion(f32[384,512]{1,0:T(8,128)S(1)} %fusion.16, bf16[384,512]{0,1:T(8,128)(2,1)S(1)} %bitcast.51, s32[512]{0:T(512)S(1)} %get-tuple-element.9, s32[512]{0:T(512)S(1)} %get-tuple-element.10), kind=kOutput, calls=%fused_computation.25 | convolution fusion | flops 1212743680 | bytes 1576960 | tf_op jit(solution)/shard_map/dot_general | solution.py:26
  163.1 3.7 %fusion.3 = bf16[1,384,2048]{2,1,0:T(8,128)(2,1)} fusion(bf16[384,512]{1,0:T(8,128)(2,1)S(1)} %fusion.12, bf16[512,2048]{1,0:T(8,128)(2,1)} %all-gather.5.cloned.1.call-done), kind=kOutput, calls=%fused_computation.7 | convolution fusion | flops 806092800 | bytes 4063232 | tf_op jit(solution)/shard_map/dot_general | solution.py:86
  (18 shorter events, 1.3 us)
Async XLA Ops:
  6.5 66.8 %copy-start.1 = (bf16[1,384,2048]{2,1,0:T(8,128)(2,1)S(1)}, bf16[1,384,2048]{2,1,0:T(8,128)(2,1)}, u32[]{:S(2)}) copy-start(bf16[1,384,2048]{2,1,0:T(8,128)(2,1)} %param.4) | copy-start | bytes 4718596
  6.5 66.8 %all-gather.3.cloned.1.call-start = ((), (), s32[]{:S(2)}) async-start(), calls=%async_computation.3 | async-start | bytes 2228224 | tf_op jit(solution)/shard_map/all_gather | solution.py:43
  10.4 152.7 %all-gather.5.cloned.1.call-start = ((), (), s32[]{:S(2)}) async-start(), calls=%async_computation.4 | async-start | bytes 2228224 | tf_op jit(solution)/shard_map/all_gather | solution.py:88
  76.9 16.0 %all-to-all-start = ((bf16[384,16,32]{0,2,1:T(8,128)(2,1)}), bf16[384,16,32]{0,2,1:T(8,128)(2,1)S(1)}, u32[]{:S(2)}, u32[]{:S(2)}) async-start(bf16[384,16,32]{0,2,1:T(8,128)(2,1)} %bitcast.3), calls=%async_computation | async-start | bytes 786432 | tf_op jit(solution)/shard_map/all_to_all | solution.py:56
  100.8 2.0 %copy-start = (f32[16,384,32]{1,0,2:T(8,128)S(1)}, f32[16,384,32]{1,0,2:T(8,128)}, u32[]{:S(2)}) copy-start(f32[16,384,32]{1,0,2:T(8,128)} %copy.17) | copy-start | bytes 2359300
  100.8 2.0 %copy-start.2 = (f32[16,384]{1,0:T(8,128)S(1)}, f32[16,384]{1,0:T(8,128)}, u32[]{:S(2)}) copy-start(f32[16,384]{1,0:T(8,128)} %get-tuple-element.7) | copy-start | bytes 73732
  100.8 2.0 %copy-start.3 = (f32[16,384]{1,0:T(8,128)S(1)}, f32[16,384]{1,0:T(8,128)}, u32[]{:S(2)}) copy-start(f32[16,384]{1,0:T(8,128)} %get-tuple-element.8) | copy-start | bytes 73732
  115.7 21.7 %all-to-all-start.1 = ((bf16[16,384,32]{1,2,0:T(8,128)(2,1)}), bf16[16,384,32]{1,2,0:T(8,128)(2,1)S(1)}, u32[]{:S(2)}, u32[]{:S(2)}) async-start(bf16[16,384,32]{1,2,0:T(8,128)(2,1)} %copy.21), calls=%async_computation.1 | async-start | bytes 786432 | tf_op jit(solution)/shard_map/all_to_all | solution.py:77
  137.3 20.8 %all-to-all-start.2 = ((bf16[16,384,32]{1,2,0:T(8,128)(2,1)}), bf16[16,384,32]{1,2,0:T(8,128)(2,1)S(1)}, u32[]{:S(2)}, u32[]{:S(2)}) async-start(bf16[16,384,32]{1,2,0:T(8,128)(2,1)} %copy.22), calls=%async_computation.2 | async-start | bytes 786432 | tf_op jit(solution)/shard_map/all_to_all | solution.py:80
Sparse Core Ops, SparseCore 0:
  10.5 62.7 all-gather.2
  76.0 69.8 all-gather.4
where the time goes:
time: 174 us
  waiting for transfers between devices  81.4 us (47%)
  matrix products  36.9 us (21%)
  starting transfers between devices  17 us (10%)
  local copies, waits for them, and re-layouts  14.3 us (8%)
  between operations  13.6 us (8%)
  blocking collectives  7.18 us (4%)
  other arithmetic  3.24 us (2%)
    all_gather x1, waiting for transfers between devices, body(): lax.all_gather(in_columns, 'row', axis=0, tiled=True)  57 us
    dot_general x6, matrix products, table_dot(): jnp.dot(matrix, values, precision=PRECISE, preferred_element_type=jnp.flo...  20.9 us
    all_to_all x1, waiting for transfers between devices, body(): lax.all_to_all(projected, 'row', split_axis=1, concat_axis=0, tiled=True)  10.8 us
    dot_general x2, matrix products, right_dot(): jnp.dot(values, matrix, precision=PRECISE, preferred_element_type=jnp.flo...  9.71 us
    all_to_all x1, starting transfers between devices, body(): lax.all_to_all(whole_imag.astype(jnp.bfloat16), 'row', split_axis=0, conc...  8.8 us
    all_to_all x1, waiting for transfers between devices, body(): lax.all_to_all(whole_imag.astype(jnp.bfloat16), 'row', split_axis=0, conc...  7.2 us
    all_to_all x1, waiting for transfers between devices, body(): lax.all_to_all(whole_real.astype(jnp.bfloat16), 'row', split_axis=0, conc...  6.31 us
    all_to_all x1, starting transfers between devices, body(): lax.all_to_all(projected, 'row', split_axis=1, concat_axis=0, tiled=True)  4.42 us
  transfers between devices with their start and end apart: 5, of which 4 were waited for; matrix products, arithmetic and copies ran while one was open for 29% of the time, Pallas kernels for 0%

commit v1 on v0

v1 whole, which is shorter than its diff:
```python
import functools
import math

import jax
import jax.numpy as jnp
import numpy as np
from jax import lax
from jax.experimental import pallas as pl
from jax.experimental.pallas import tpu as pltpu
from jax.sharding import PartitionSpec as P

GS = 64
EPS = 1e-06
LANES = 128
F32 = jnp.float32
BF16 = jnp.bfloat16


def angles(left, right, modulus):
    product = np.arange(left)[:, None] * np.arange(right)[None, :] % modulus
    radians = product * (2.0 * math.pi / modulus)
    return np.cos(radians), np.sin(radians)


def channel_tables(narrow):
    cos, sin = angles(GS, GS, GS)
    half = narrow // 2
    forward = np.zeros((GS, GS))
    combine = np.zeros((GS, GS))
    for slot in range(GS):
        owner, place = divmod(slot, narrow)
        j = owner * half + place % half
        if place >= half and j > 0:
            forward[slot] = sin[j]
            combine[slot, j] = -1.0
            combine[slot, GS - j] = 1.0
        else:
            j = GS // 2 if place >= half else j
            forward[slot] = cos[j]
            combine[slot, j] = 1.0
            combine[slot, (GS - j) % GS] = 1.0
    copies = np.eye(LANES // GS)
    return np.kron(copies, forward), np.kron(copies, combine)


def tables(peers, rows, channels):
    narrow = channels // peers
    step = rows // peers
    length = peers * rows
    forward, combine = channel_tables(narrow)
    cos, sin = angles(peers, peers, peers)
    eye = np.eye(narrow)
    chunk = LANES // narrow
    first = np.concatenate(
        [
            np.kron(part[t : t + chunk], eye)
            for t in range(0, peers, chunk)
            for part in (cos, -sin)
        ]
    )
    turn = np.stack(angles(peers, rows, length)) / math.sqrt(length * GS)
    second = np.concatenate(angles(rows, rows, rows), axis=1)
    order = np.zeros((rows, rows))
    for t in range(peers):
        for u in range(step):
            order[u * peers + t, t * step + u] = 1.0
    return (
        jnp.asarray(forward, BF16),
        jnp.asarray(combine, BF16),
        jnp.asarray(first, BF16),
        jnp.asarray(turn, F32),
        jnp.asarray(second, BF16),
        jnp.asarray(order, BF16),
    )


def dot(a, b):
    return jnp.dot(a, b, preferred_element_type=F32)


def dot_nt(a, b):
    return lax.dot_general(a, b, (((1,), (1,)), ((), ())), preferred_element_type=F32)


def kernel(
    peers,
    cols,
    tokens_hbm,
    gain_ref,
    in_ref,
    out_w_ref,
    forward_ref,
    combine_ref,
    first_hbm,
    turn_hbm,
    second_hbm,
    order_hbm,
    result_ref,
    tokens,
    first,
    turn,
    second,
    order,
    normed,
    projected,
    w_in,
    w_out,
    send_one,
    got_one,
    lines,
    send_two,
    got_two,
    arranged,
    local_sem,
    g_send,
    g_recv,
    c_send,
    c_recv,
    x_send,
    x_recv,
):
    me = lax.axis_index("row")
    core = lax.axis_index("col")
    rows, width = tokens.shape
    channels = projected.shape[1]
    narrow = channels // peers
    half = narrow // 2
    step = rows // peers

    loads = [
        pltpu.make_async_copy(src, dst, local_sem.at[i])
        for i, (src, dst) in enumerate(
            (
                (tokens_hbm, tokens),
                (first_hbm, first),
                (turn_hbm, turn),
                (second_hbm, second),
                (order_hbm, order),
            )
        )
    ]
    for load in loads:
        load.start()

    def peer(o):
        return lax.rem(me + o, peers)

    def mate(o):
        return lax.rem(core + o, cols)

    barrier = pltpu.get_barrier_semaphore()
    for o in range(1, peers):
        pl.semaphore_signal(barrier, inc=1, device_id={"row": peer(o)})
    for o in range(1, cols):
        pl.semaphore_signal(barrier, inc=1, device_id={"col": mate(o)})
    pl.semaphore_wait(barrier, peers - 1 + cols - 1)

    def spread(which, src, buffer):
        copies = []
        for o in range(1, peers):
            copy = pltpu.make_async_remote_copy(
                src_ref=src,
                dst_ref=buffer.at[core, me],
                send_sem=g_send.at[which, o],
                recv_sem=g_recv.at[which, o],
                device_id={"row": peer(o)},
            )
            copy.start()
            copies.append(copy)
        own = pltpu.make_async_copy(src, buffer.at[core, me], g_send.at[which, 0])
        own.start()
        return copies, own

    def relay(which, buffer, copies, own):
        for copy in copies:
            copy.wait_recv()
        own.wait()
        passed = []
        for o in range(1, cols):
            copy = pltpu.make_async_remote_copy(
                src_ref=buffer.at[core],
                dst_ref=buffer.at[core],
                send_sem=c_send.at[which, o],
                recv_sem=c_recv.at[which, o],
                device_id={"col": mate(o)},
            )
            copy.start()
            passed.append(copy)
        return passed

    in_copies, in_own = spread(0, in_ref, w_in)

    loads[0].wait()
    gain = gain_ref[...].astype(F32)
    tile = 32

    def norm(i, carry):
        at = pl.ds(pl.multiple_of(i * tile, tile), tile)
        block = tokens[at, :].astype(F32)
        inverse = lax.rsqrt(jnp.mean(block * block, axis=-1, keepdims=True) + EPS)
        normed[at, :] = (block * inverse * gain).astype(BF16)
        return carry

    lax.fori_loop(0, rows // tile, norm, 0)

    in_passed = relay(0, w_in, in_copies, in_own)
    out_copies, out_own = spread(1, out_w_ref, w_out)
    for copy in in_passed:
        copy.wait_recv()

    part = channels // cols
    for c in range(cols):
        projected[:, c * part : (c + 1) * part] = dot(
            normed[...], w_in[c].reshape(width, part)
        ).astype(BF16)

    for b in range(0, channels, LANES):
        slots = dot_nt(forward_ref[...], projected[:, b : b + LANES]).astype(BF16)
        send_one[b // narrow : (b + LANES) // narrow] = slots.reshape(
            LANES // narrow, narrow, rows
        )

    def exchange(which, src, dst):
        copies = []
        for o in range(1, peers):
            copy = pltpu.make_async_remote_copy(
                src_ref=src.at[peer(o)],
                dst_ref=dst.at[me],
                send_sem=x_send.at[which, o],
                recv_sem=x_recv.at[which, o],
                device_id={"row": peer(o)},
            )
            copy.start()
            copies.append(copy)
        own = pltpu.make_async_copy(src.at[me], dst.at[me], x_send.at[which, 0])
        own.start()
        for copy in copies:
            copy.wait_recv()
        own.wait()
        return copies

    one_copies = exchange(0, send_one, got_one)
    for load in loads[1:]:
        load.wait()
    columns = got_one[...].reshape(channels, rows)
    place = lax.broadcasted_iota(jnp.int32, (narrow, rows), 0)
    leads = lax.rem(me * narrow, GS) == 0
    first_sine = jnp.where(leads, half + 1, half)
    sine = place >= first_sine
    chunk = LANES // narrow
    for t0 in range(0, peers, chunk):
        both = dot(first[2 * t0 * narrow : 2 * (t0 + chunk) * narrow, :], columns)
        for i in range(chunk):
            t = t0 + i
            real = both[i * narrow : (i + 1) * narrow]
            imag = both[LANES + i * narrow : LANES + (i + 1) * narrow]
            cos = turn[0, t : t + 1, :]
            sin = turn[1, t : t + 1, :]
            z_real = real * cos + imag * sin
            z_imag = imag * cos - real * sin
            at = slice(t * narrow, (t + 1) * narrow)
            lines[at, :rows] = jnp.where(sine, -z_imag, z_real)
            lines[at, rows:] = jnp.where(sine, z_real, z_imag)
    whole = dot_nt(second[...], lines[...].astype(BF16))
    send_two[...] = whole.reshape(peers, step, channels).astype(BF16)
    two_copies = exchange(1, send_two, got_two)

    out_passed = relay(1, w_out, out_copies, out_own)

    block_of = lax.broadcasted_iota(jnp.int32, (step, LANES), 1) // narrow
    for d0 in range(0, peers, chunk):
        for t0 in range(0, peers, chunk):
            held = [
                got_two[d0 + i, :, t0 * narrow : (t0 + chunk) * narrow].astype(F32)
                for i in range(chunk)
            ]
            for j in range(chunk):
                made = None
                for i in range(chunk):
                    shift = (i - j) * narrow % LANES
                    moved = pltpu.roll(held[i], shift, 1) if shift else held[i]
                    made = moved if made is None else jnp.where(block_of == i, moved, made)
                t = t0 + j
                arranged[t * step : (t + 1) * step, d0 * narrow : (d0 + chunk) * narrow] = made
    natural = dot(order[...], arranged[...].astype(BF16)).astype(BF16)
    mixed = jnp.concatenate(
        [
            dot(natural[:, b : b + LANES], combine_ref[...]).astype(BF16)
            for b in range(0, channels, LANES)
        ],
        axis=1,
    )
    for copy in out_passed:
        copy.wait_recv()
    wide = w_out.shape[3]
    group = max(1, 256 // wide)
    for p in range(0, peers, group):
        weight = jnp.concatenate(
            [w_out[:, p + i].reshape(channels, wide) for i in range(group)], axis=1
        )
        result_ref[:, p * wide : (p + group) * wide] = dot(mixed, weight).astype(BF16)

    for copy in in_copies + in_passed + out_copies + out_passed + one_copies + two_copies:
        copy.wait_send()


def body(peers, cols, tokens, norm_gain, in_weight, out_weight):
    rows, width = tokens.shape[1:]
    in_rows, in_cols = in_weight.shape
    out_rows, out_cols = out_weight.shape
    channels = in_cols * cols
    narrow = channels // peers
    step = rows // peers
    forward, combine, first, turn, second, order = tables(peers, rows, channels)
    vmem = pl.BlockSpec(memory_space=pltpu.VMEM)
    hbm = pl.BlockSpec(memory_space=pl.ANY)
    result = pl.pallas_call(
        functools.partial(kernel, peers, cols),
        out_shape=jax.ShapeDtypeStruct((rows, width), BF16),
        in_specs=[hbm, vmem, vmem, vmem, vmem, vmem, hbm, hbm, hbm, hbm],
        out_specs=vmem,
        scratch_shapes=[
            pltpu.VMEM((rows, width), BF16),
            pltpu.VMEM(first.shape, BF16),
            pltpu.VMEM(turn.shape, F32),
            pltpu.VMEM(second.shape, BF16),
            pltpu.VMEM(order.shape, BF16),
            pltpu.VMEM((rows, width), BF16),
            pltpu.VMEM((rows, channels), BF16),
            pltpu.VMEM((cols, peers, in_rows, in_cols), BF16),
            pltpu.VMEM((cols, peers, out_rows, out_cols), BF16),
            pltpu.VMEM((peers, narrow, rows), BF16),
            pltpu.VMEM((peers, narrow, rows), BF16),
            pltpu.VMEM((channels, 2 * rows), F32),
            pltpu.VMEM((peers, step, channels), BF16),
            pltpu.VMEM((peers, step, channels), BF16),
            pltpu.VMEM((rows, channels), F32),
            pltpu.SemaphoreType.DMA((5,)),
            pltpu.SemaphoreType.DMA((2, peers)),
            pltpu.SemaphoreType.DMA((2, peers)),
            pltpu.SemaphoreType.DMA((2, cols)),
            pltpu.SemaphoreType.DMA((2, cols)),
            pltpu.SemaphoreType.DMA((2, peers)),
            pltpu.SemaphoreType.DMA((2, peers)),
        ],
        compiler_params=pltpu.CompilerParams(
            collective_id=0, has_side_effects=True, vmem_limit_bytes=60 * 1024 * 1024
        ),
    )(tokens[0], norm_gain[None], in_weight, out_weight, forward, combine, first, turn, second, order)
    return result[None]


def solution(mesh):
    in_specs = (P("col", "row", None), P(), P("row", "col"), P("col", "row"))
    out_specs = P("col", "row", None)
    step = functools.partial(body, mesh.shape["row"], mesh.shape["col"])
    return jax.shard_map(step, mesh=mesh, in_specs=in_specs, out_specs=out_specs, check_vma=False)
```

time: 174 us -> 93.7 us (0.54)
  the two profiles are of different devices: /device:TPU:0 before, /device:TPU:17 now
where the time goes in v1:
time: 93.7 us; the launch traced here: 93.5 us
  Pallas kernels  89.5 us (96%)
  local copies, waits for them, and re-layouts  4.02 us (4%)
    pallas_call x1, Pallas kernels, body(): pl.pallas_call(functools.partial(kernel, peers, cols), out_shape=jax.Shap...  89.5 us
    unnamed x1, local copies, waits for them, and re-layouts  2.73 us

profile of v1, /device:TPU:17, one launch (start us, length us, event | category | flops | bytes accessed | tf_op | source)
XLA Modules:
  0.0 93.5 jit_solution(8451208805354394172)
XLA Ops:
  0.0 1.3 %broadcast_in_dim.6.gain_ref = bf16[1,2048]{1,0:T(2,128)(2,1)} reshape(bf16[2048]{0:T(1024)(128)(2,1)} %param.11) | data formatting | bytes 8192 | tf_op jit(solution)/shard_map/broadcast_in_dim | solution.py:349
  1.3 89.5 %shard_map.100 = bf16[384,2048]{1,0:T(8,128)(2,1)} custom-call(bf16[384,2048]{1,0:T(8,128)(2,1)} %bitcast.3, bf16[1,2048]{1,0:T(2,128)(2,1)} %broadcast_in_dim.6.gain_ref, bf16[128,256]{1,0:T(8,128)(2,1)} %in_ref.1, bf16[256,128]{1,0:T(8,128)(2,1)} %out_w_ref.1, bf16[128,128]{1,0:T(8,128)(2,1)} %constant.12.clone.forward_ref, ...), custom_call_target="tpu_custom_call" | custom-call | tf_op jit(solution)/shard_map/pallas_call | solution.py:317
  90.8 2.7 %copy.12 = bf16[1,384,2048]{2,1,0:T(8,128)(2,1)} copy(bf16[1,384,2048]{2,1,0:T(8,128)(2,1)} %bitcast.2) | data formatting | bytes 3145728

commit v2 on v1

--- a/solution.py
+++ b/solution.py
@@ -72,6 +72,16 @@
         jnp.asarray(second, BF16),
         jnp.asarray(order, BF16),
     )
+
+
+def gather_orders(peers):
+    short = []
+    stride, rest = 1, peers
+    while len(short) < 2 and rest % 2 == 0:
+        short.append((stride, 2))
+        stride, rest = stride * 2, rest // 2
+    long = [(stride, rest)] if rest > 1 else []
+    return [long + short, long + short[::-1]]
 
 
 def dot(a, b):
@@ -112,6 +122,7 @@
     got_two,
     arranged,
     local_sem,
+    own_sem,
     g_send,
     g_recv,
     c_send,
@@ -122,7 +133,10 @@
     me = lax.axis_index("row")
     core = lax.axis_index("col")
     rows, width = tokens.shape
-    channels = projected.shape[1]
+    channels = first.shape[1]
+    parts = g_send.shape[1]
+    orders = gather_orders(peers)
+    stages = len(orders[0])
     narrow = channels // peers
     half = narrow // 2
     step = rows // peers
@@ -155,43 +169,80 @@
         pl.semaphore_signal(barrier, inc=1, device_id={"col": mate(o)})
     pl.semaphore_wait(barrier, peers - 1 + cols - 1)
 
-    def spread(which, src, buffer):
-        copies = []
-        for o in range(1, peers):
-            copy = pltpu.make_async_remote_copy(
-                src_ref=src,
-                dst_ref=buffer.at[core, me],
-                send_sem=g_send.at[which, o],
-                recv_sem=g_recv.at[which, o],
-                device_id={"row": peer(o)},
-            )
-            copy.start()
-            copies.append(copy)
-        own = pltpu.make_async_copy(src, buffer.at[core, me], g_send.at[which, 0])
-        own.start()
-        return copies, own
-
-    def relay(which, buffer, copies, own):
-        for copy in copies:
-            copy.wait_recv()
-        own.wait()
-        passed = []
-        for o in range(1, cols):
-            copy = pltpu.make_async_remote_copy(
-                src_ref=buffer.at[core],
-                dst_ref=buffer.at[core],
-                send_sem=c_send.at[which, o],
-                recv_sem=c_recv.at[which, o],
-                device_id={"col": mate(o)},
-            )
-            copy.start()
-            passed.append(copy)
-        return passed
-
-    in_copies, in_own = spread(0, in_ref, w_in)
+    class Gather:
+        def __init__(self, which, src, buffer):
+            self.which, self.src, self.buffer = which, src, buffer
+            self.height = src.shape[0] // parts
+            self.held = [[None] for _ in range(parts)]
+            self.open = [[] for _ in range(parts)]
+            self.sent = []
+            self.count = [0] * parts
+            self.own = pltpu.make_async_copy(src, buffer.at[core, me], own_sem.at[which])
+            self.own.start()
+
+        def issue(self, part, stage):
+            stride, size = orders[part % len(orders)][stage]
+            at = pl.ds(part * self.height, self.height)
+            place = lax.rem(lax.div(me, stride), size)
+            arrived = []
+            for o in range(1, size):
+                to = me + (lax.rem(place + o, size) - place) * stride
+                origin = (lax.rem(place + size - o, size) - place) * stride
+                for held in self.held[part]:
+                    block = me if held is None else held
+                    copy = pltpu.make_async_remote_copy(
+                        src_ref=self.src.at[at]
+                        if held is None
+                        else self.buffer.at[core, block, at],
+                        dst_ref=self.buffer.at[core, block, at],
+                        send_sem=g_send.at[self.which, part, self.count[part]],
+                        recv_sem=g_recv.at[self.which, part, self.count[part]],
+                        device_id={"row": to},
+                    )
+                    copy.start()
+                    self.count[part] += 1
+                    self.open[part].append(copy)
+                    self.sent.append(copy)
+                    arrived.append(block + origin)
+            self.held[part] += arrived
+
+        def wait(self, part):
+            for copy in self.open[part]:
+                copy.wait_recv()
+            self.open[part] = []
+
+        def advance(self, stage):
+            for part in range(parts):
+                self.wait(part)
+                self.issue(part, stage)
+
+        def relay(self):
+            self.own.wait()
+            self.passed = []
+            for part in range(parts):
+                self.wait(part)
+                at = pl.ds(part * self.height, self.height)
+                for o in range(1, cols):
+                    copy = pltpu.make_async_remote_copy(
+                        src_ref=self.buffer.at[core, :, at],
+                        dst_ref=self.buffer.at[core, :, at],
+                        send_sem=c_send.at[self.which, part, o],
+                        recv_sem=c_recv.at[self.which, part, o],
+                        device_id={"col": mate(o)},
+                    )
+                    copy.start()
+                    self.passed.append(copy)
+
+        def finish(self):
+            for copy in self.passed:
+                copy.wait_recv()
+
+    gather_in = Gather(0, in_ref, w_in)
+    gather_out = Gather(1, out_w_ref, w_out)
+    gather_in.advance(0)
 
     loads[0].wait()
-    gain = gain_ref[...].astype(F32)
+    gain = gain_ref[...].astype(F32).reshape(1, width)
     tile = 32
 
     def norm(i, carry):
@@ -203,19 +254,21 @@
 
     lax.fori_loop(0, rows // tile, norm, 0)
 
-    in_passed = relay(0, w_in, in_copies, in_own)
-    out_copies, out_own = spread(1, out_w_ref, w_out)
-    for copy in in_passed:
-        copy.wait_recv()
+    for stage in range(1, stages):
+        gather_in.advance(stage)
+    gather_out.advance(0)
+    gather_in.relay()
 
     part = channels // cols
-    for c in range(cols):
-        projected[:, c * part : (c + 1) * part] = dot(
-            normed[...], w_in[c].reshape(width, part)
-        ).astype(BF16)
-
+    for i in range(cols):
+        if i == 1:
+            gather_in.finish()
+        c = mate(i)
+        projected[c] = dot(normed[...], w_in[c].reshape(width, part)).astype(BF16)
+
+    natural_channels = jnp.concatenate([projected[c] for c in range(cols)], axis=1)
     for b in range(0, channels, LANES):
-        slots = dot_nt(forward_ref[...], projected[:, b : b + LANES]).astype(BF16)
+        slots = dot_nt(forward_ref[...], natural_channels[:, b : b + LANES]).astype(BF16)
         send_one[b // narrow : (b + LANES) // narrow] = slots.reshape(
             LANES // narrow, narrow, rows
         )
@@ -234,12 +287,19 @@
             copies.append(copy)
         own = pltpu.make_async_copy(src.at[me], dst.at[me], x_send.at[which, 0])
         own.start()
+        return copies, own
+
+    def land(copies, own):
         for copy in copies:
             copy.wait_recv()
         own.wait()
-        return copies
-
-    one_copies = exchange(0, send_one, got_one)
+
+    one_copies, one_own = exchange(0, send_one, got_one)
+    if stages > 1:
+        gather_out.advance(1)
+    land(one_copies, one_own)
+    for stage in range(2, stages):
+        gather_out.advance(stage)
     for load in loads[1:]:
         load.wait()
     columns = got_one[...].reshape(channels, rows)
@@ -263,9 +323,9 @@
             lines[at, rows:] = jnp.where(sine, z_real, z_imag)
     whole = dot_nt(second[...], lines[...].astype(BF16))
     send_two[...] = whole.reshape(peers, step, channels).astype(BF16)
-    two_copies = exchange(1, send_two, got_two)
-
-    out_passed = relay(1, w_out, out_copies, out_own)
+    two_copies, two_own = exchange(1, send_two, got_two)
+    gather_out.relay()
+    land(two_copies, two_own)
 
     block_of = lax.broadcasted_iota(jnp.int32, (step, LANES), 1) // narrow
     for d0 in range(0, peers, chunk):
@@ -290,8 +350,7 @@
         ],
         axis=1,
     )
-    for copy in out_passed:
-        copy.wait_recv()
+    gather_out.finish()
     wide = w_out.shape[3]
     group = max(1, 256 // wide)
     for p in range(0, peers, group):
@@ -300,7 +359,14 @@
         )
         result_ref[:, p * wide : (p + group) * wide] = dot(mixed, weight).astype(BF16)
 
-    for copy in in_copies + in_passed + out_copies + out_passed + one_copies + two_copies:
+    for copy in (
+        gather_in.sent
+        + gather_in.passed
+        + gather_out.sent
+        + gather_out.passed
+        + one_copies
+        + two_copies
+    ):
         copy.wait_send()
 
 
@@ -311,6 +377,7 @@
     channels = in_cols * cols
     narrow = channels // peers
     step = rows // peers
+    parts = max(1, min(4, in_rows // 16, out_rows // 16))
     forward, combine, first, turn, second, order = tables(peers, rows, channels)
     vmem = pl.BlockSpec(memory_space=pltpu.VMEM)
     hbm = pl.BlockSpec(memory_space=pl.ANY)
@@ -326,7 +393,7 @@
             pltpu.VMEM(second.shape, BF16),
             pltpu.VMEM(order.shape, BF16),
             pltpu.VMEM((rows, width), BF16),
-            pltpu.VMEM((rows, channels), BF16),
+            pltpu.VMEM((cols, rows, in_cols), BF16),
             pltpu.VMEM((cols, peers, in_rows, in_cols), BF16),
             pltpu.VMEM((cols, peers, out_rows, out_cols), BF16),
             pltpu.VMEM((peers, narrow, rows), BF16),
@@ -336,17 +403,18 @@
             pltpu.VMEM((peers, step, channels), BF16),
             pltpu.VMEM((rows, channels), F32),
             pltpu.SemaphoreType.DMA((5,)),
-            pltpu.SemaphoreType.DMA((2, peers)),
-            pltpu.SemaphoreType.DMA((2, peers)),
-            pltpu.SemaphoreType.DMA((2, cols)),
-            pltpu.SemaphoreType.DMA((2, cols)),
+            pltpu.SemaphoreType.DMA((2,)),
+            pltpu.SemaphoreType.DMA((2, parts, peers)),
+            pltpu.SemaphoreType.DMA((2, parts, peers)),
+            pltpu.SemaphoreType.DMA((2, parts, cols)),
+            pltpu.SemaphoreType.DMA((2, parts, cols)),
             pltpu.SemaphoreType.DMA((2, peers)),
             pltpu.SemaphoreType.DMA((2, peers)),
         ],
         compiler_params=pltpu.CompilerParams(
             collective_id=0, has_side_effects=True, vmem_limit_bytes=60 * 1024 * 1024
         ),
-    )(tokens[0], norm_gain[None], in_weight, out_weight, forward, combine, first, turn, second, order)
+    )(tokens[0], norm_gain, in_weight, out_weight, forward, combine, first, turn, second, order)
     return result[None]
 
 

time: 93.7 us -> 55.7 us (0.59)
  the two profiles are of different devices: /device:TPU:17 before, /device:TPU:0 now
where the time goes in v2:
time: 55.7 us; the launch traced here: 55.5 us
  Pallas kernels  52.8 us (95%)
  local copies, waits for them, and re-layouts  2.73 us (5%)
    pallas_call x1, Pallas kernels, body(): pl.pallas_call(functools.partial(kernel, peers, cols), out_shape=jax.Shap...  52.8 us
    unnamed x1, local copies, waits for them, and re-layouts  2.73 us

profile of v2, /device:TPU:0, one launch (start us, length us, event | category | flops | bytes accessed | tf_op | source)
XLA Modules:
  0.0 55.5 jit_solution(15538448167528330514)
XLA Ops:
  0.0 52.8 %shard_map.100 = bf16[384,2048]{1,0:T(8,128)(2,1)} custom-call(bf16[384,2048]{1,0:T(8,128)(2,1)} %bitcast.3, bf16[2048]{0:T(1024)(128)(2,1)} %gain_ref.1, bf16[128,256]{1,0:T(8,128)(2,1)} %in_ref.1, bf16[256,128]{1,0:T(8,128)(2,1)} %out_w_ref.1, bf16[128,128]{1,0:T(8,128)(2,1)} %constant.12.clone.forward_ref, bf16[128,128]{1,0:T(8,128)(2,1)} %constant.13.clone.combine_ref, ...), custom_call_target="tpu_custom_call" | custom-call | tf_op jit(solution)/shard_map/pallas_call | solution.py:384
  52.8 2.7 %copy.12 = bf16[1,384,2048]{2,1,0:T(8,128)(2,1)} copy(bf16[1,384,2048]{2,1,0:T(8,128)(2,1)} %bitcast.2) | data formatting | bytes 3145728

commit v3 on v2

--- a/solution.py
+++ b/solution.py
@@ -106,6 +106,7 @@
     second_hbm,
     order_hbm,
     result_ref,
+    result,
     tokens,
     first,
     turn,
@@ -123,6 +124,7 @@
     arranged,
     local_sem,
     own_sem,
+    store_sem,
     g_send,
     g_recv,
     c_send,
@@ -252,10 +254,12 @@
         normed[at, :] = (block * inverse * gain).astype(BF16)
         return carry
 
-    lax.fori_loop(0, rows // tile, norm, 0)
-
-    for stage in range(1, stages):
-        gather_in.advance(stage)
+    tiles = rows // tile
+    cuts = [tiles * i // stages for i in range(stages + 1)]
+    for stage in range(stages):
+        if stage:
+            gather_in.advance(stage)
+        lax.fori_loop(cuts[stage], cuts[stage + 1], norm, 0)
     gather_out.advance(0)
     gather_in.relay()
 
@@ -351,13 +355,20 @@
         axis=1,
     )
     gather_out.finish()
+    stores = []
     wide = w_out.shape[3]
     group = max(1, 256 // wide)
     for p in range(0, peers, group):
         weight = jnp.concatenate(
             [w_out[:, p + i].reshape(channels, wide) for i in range(group)], axis=1
         )
-        result_ref[:, p * wide : (p + group) * wide] = dot(mixed, weight).astype(BF16)
+        at = slice(p * wide, (p + group) * wide)
+        result[:, at] = dot(mixed, weight).astype(BF16)
+        store = pltpu.make_async_copy(result.at[:, at], result_ref.at[:, at], store_sem.at[p])
+        store.start()
+        stores.append(store)
+    for store in stores:
+        store.wait()
 
     for copy in (
         gather_in.sent
@@ -385,8 +396,9 @@
         functools.partial(kernel, peers, cols),
         out_shape=jax.ShapeDtypeStruct((rows, width), BF16),
         in_specs=[hbm, vmem, vmem, vmem, vmem, vmem, hbm, hbm, hbm, hbm],
-        out_specs=vmem,
+        out_specs=hbm,
         scratch_shapes=[
+            pltpu.VMEM((rows, width), BF16),
             pltpu.VMEM((rows, width), BF16),
             pltpu.VMEM(first.shape, BF16),
             pltpu.VMEM(turn.shape, F32),
@@ -404,6 +416,7 @@
             pltpu.VMEM((rows, channels), F32),
             pltpu.SemaphoreType.DMA((5,)),
             pltpu.SemaphoreType.DMA((2,)),
+            pltpu.SemaphoreType.DMA((peers,)),
             pltpu.SemaphoreType.DMA((2, parts, peers)),
             pltpu.SemaphoreType.DMA((2, parts, peers)),
             pltpu.SemaphoreType.DMA((2, parts, cols)),

time: 55.7 us -> 55.6 us (level)
  no operation moved by 1% of the time
where the time goes in v3:
time: 55.6 us; the launch traced here: 55.4 us
  Pallas kernels  52.6 us (95%)
  local copies, waits for them, and re-layouts  2.73 us (5%)
    pallas_call x1, Pallas kernels, body(): pl.pallas_call(functools.partial(kernel, peers, cols), out_shape=jax.Shap...  52.6 us
    unnamed x1, local copies, waits for them, and re-layouts  2.73 us

profile of v3, /device:TPU:0, one launch (start us, length us, event | category | flops | bytes accessed | tf_op | source)
XLA Modules:
  0.0 55.4 jit_solution(17337185744508866284)
XLA Ops:
  0.0 52.6 %shard_map.100 = bf16[384,2048]{1,0:T(8,128)(2,1)} custom-call(bf16[384,2048]{1,0:T(8,128)(2,1)} %bitcast.3, bf16[2048]{0:T(1024)(128)(2,1)} %gain_ref.1, bf16[128,256]{1,0:T(8,128)(2,1)} %in_ref.1, bf16[256,128]{1,0:T(8,128)(2,1)} %out_w_ref.1, bf16[128,128]{1,0:T(8,128)(2,1)} %constant.12.clone.forward_ref, bf16[128,128]{1,0:T(8,128)(2,1)} %constant.13.clone.combine_ref, ...), custom_call_target="tpu_custom_call" | custom-call | tf_op jit(solution)/shard_map/pallas_call | solution.py:395
  52.7 2.7 %copy.12 = bf16[1,384,2048]{2,1,0:T(8,128)(2,1)} copy(bf16[1,384,2048]{2,1,0:T(8,128)(2,1)} %bitcast.2) | data formatting | bytes 3145728
